TPU v7x, 128 devices: a whole 4x4x4 slice. The times are simulated.
128 devices in a mesh: sp: 16 (over z, y), fs: 4 (over x), tp: 2 (over core).
Axes of the slice: x: 4, y: 4, z: 4, core: 2. Of those that a mesh axis runs over, the one named last changes fastest.
Arguments:
- tokens: bfloat16 [4, 4096, 2048], P('fs', 'sp', 'tp'), may hold values from -6 to 6
- norm_gain: float32 [2048], replicated, may hold values from 0.1 to 1.9
- lin_query: bfloat16 [2048, 1024], P(None, ('fs', 'tp')), may hold values from -0.125 to 0.125
- lin_key: bfloat16 [2048, 1024], P(None, ('fs', 'tp')), may hold values from -0.125 to 0.125
- lin_value: bfloat16 [2048, 2048], P(None, ('fs', 'tp')), may hold values from -0.125 to 0.125
- lin_decay: bfloat16 [2048, 1024], P(None, ('fs', 'tp')), may hold values from -0.125 to 0.125
- decay_bias: float32 [1024], replicated, may hold values from -0.5 to 8.5
- decay_shift: bfloat16 [2, 4, 4096], P(None, 'fs', 'sp'), may hold values from -1.4 to 1.5, as said below
- soft_query: bfloat16 [2048, 2048], P(None, ('fs', 'tp')), may hold values from -0.190034947 to 0.190034947
- soft_key: bfloat16 [2048, 2048], P(None, ('fs', 'tp')), may hold values from -1.9887378 to 1.9887378
- soft_value: bfloat16 [2048, 2048], P(None, ('fs', 'tp')), may hold values from -0.125 to 0.125
- soft_lambda: float32 [8], replicated, may hold values from 0.3 to 0.8
- lin_gain: float32 [256], replicated, may hold values from 0.1 to 1.9
- soft_gain: float32 [256], replicated, may hold values from 0.1 to 1.9
- lin_out: bfloat16 [2048, 2048], P(('fs', 'tp')), may hold values from -0.09375 to 0.09375
- soft_out: bfloat16 [2048, 2048], P(('fs', 'tp')), may hold values from -0.09375 to 0.09375
Outputs:
- mixed: bfloat16 [4, 4096, 2048], P('fs', 'sp', 'tp')
- log_mass: float32 [8, 2, 4, 4096], P(('fs', 'tp'), None, None, 'sp')
Inputs may be any that keep to these rules, and one draw needn't show every extreme that they name: `decay_shift`: row 1 is never positive.
All inputs are finite; a program needn't handle non-finite values.
Results may differ from a plain program's by a relative error of at most 0.02.
Values may be sent and summed in bfloat16 or wider, within the bound.
No kernel may reach another device: no remote copies, remote signals or barrier semaphores. Data moves between devices by JAX's collectives and lax.ppermute only.
A program may use at most 192 MiB of HBM per device.

v0:
```python
import jax
import jax.numpy as jnp
from jax import lax
from jax.sharding import Mesh
from jax.sharding import PartitionSpec as P

GLA_KEY = 128
GLA_VALUE = 256
DIFF_HEAD = 128
DIFF_VALUE = 256
BLOCK = 64
SP = ("sp_0", "sp_1")
norm_eps = 1e-06
decay_tau = 16.0
rope_base = 500000.0


def neutral_like(array, identity):
    return jax.tree.map(
        lambda a, e: jnp.broadcast_to(jnp.asarray(e, a.dtype), a.shape), array, identity
    )


def carried_in(array, axes, combine, identity):
    before = start = neutral_like(array, identity)
    running = array
    for axis in reversed(axes):
        length, place = (lax.axis_size(axis), lax.axis_index(axis))
        pieces = jax.tree.map(
            lambda part, kind: lax.all_gather(part.astype(kind), axis),
            running,
            (jnp.bfloat16, jnp.bfloat16),
        )
        inside, running = (start, start)
        for k in range(length):
            passed = k < place
            running = combine(
                running, jax.tree.map(lambda part, own: part[k].astype(own.dtype), pieces, array)
            )
            inside = jax.tree.map(lambda new, old: jnp.where(passed, new, old), running, inside)
        before = combine(inside, before)
    return before


def scaled_rms(values, norm_gain):
    return (
        values * lax.rsqrt(jnp.mean(values * values, axis=-1, keepdims=True) + norm_eps) * norm_gain
    )


def rotate(values, positions):
    half_dim = values.shape[-1] // 2
    inv_freq = jnp.power(
        jnp.float32(rope_base), -jnp.arange(half_dim, dtype=jnp.float32) * (2.0 / values.shape[-1])
    )
    angles = positions.astype(jnp.float32)[:, None] * inv_freq[None, :]
    cos_table = jnp.cos(angles)[:, None, None, :]
    sin_table = jnp.sin(angles)[:, None, None, :]
    widened = values.astype(jnp.float32)
    first_half = widened[..., :half_dim]
    second_half = widened[..., half_dim:]
    turned = jnp.concatenate(
        [
            first_half * cos_table - second_half * sin_table,
            second_half * cos_table + first_half * sin_table,
        ],
        axis=-1,
    )
    return turned.astype(jnp.bfloat16)


def block_pass(queries, key_rows, value_rows, log_decay, block_len):
    groups, length, heads, key_dim = queries.shape
    value_dim = value_rows.shape[-1]
    block_count = length // block_len

    def split(tensor):
        return tensor.reshape(groups, block_count, block_len, heads, tensor.shape[-1]).transpose(
            1, 0, 3, 2, 4
        )

    causal = jnp.tril(jnp.ones((block_len, block_len), dtype=bool))[:, :, None]

    def advance(carry, inputs):
        state_now, offset = carry
        query_blk, key_blk, value_blk, decay_blk = inputs
        cum_log = jnp.cumsum(decay_blk, axis=2)
        inner_part = jnp.einsum("bhcd,bhdv->bhcv", query_blk * jnp.exp(cum_log), state_now)
        decay_pair = jnp.exp(
            jnp.where(causal, cum_log[:, :, :, None, :] - cum_log[:, :, None, :, :], -jnp.inf)
        )
        scores = jnp.sum(
            query_blk[:, :, :, None, :] * key_blk[:, :, None, :, :] * decay_pair, axis=-1
        )
        local_part = jnp.einsum("bhij,bhjv->bhiv", scores, value_blk)
        last_log = cum_log[:, :, -1, :]
        state_now = jnp.exp(last_log)[..., None] * state_now + jnp.einsum(
            "bhcd,bhcv->bhdv", key_blk * jnp.exp(last_log[:, :, None, :] - cum_log), value_blk
        )
        carried = query_blk * jnp.exp(offset[:, :, None, :] + cum_log)
        return ((state_now, offset + last_log), (inner_part + local_part, carried))

    start = (
        jnp.zeros((groups, heads, key_dim, value_dim), jnp.float32),
        jnp.zeros((groups, heads, key_dim), jnp.float32),
    )
    (state_end, offset_end), (outs, carried) = lax.scan(
        advance, start, (split(queries), split(key_rows), split(value_rows), split(log_decay))
    )
    return (outs, carried, state_end, offset_end)


def project(rows, weight):
    lead_shape = rows.shape[:-1]
    flat_rows = rows.reshape(-1, rows.shape[-1])
    product = jnp.dot(flat_rows, weight, preferred_element_type=jnp.float32)
    return product.reshape(lead_shape + (weight.shape[1],))


def chain_join(earlier, later):
    return (earlier[0] * later[0], later[0][..., None] * earlier[1] + later[1])


def attend(queries, query_pos, reach, all_keys, all_values, soft_lambda, soft_gain, rows_dev):
    groups, query_rows, soft_heads = queries.shape[:3]
    block_total = all_keys.shape[1] // rows_dev
    scale = DIFF_HEAD ** (-0.5)

    def first_pass(block_id, carry):
        top_now, total_now, score_store = carry
        key_blk = lax.dynamic_slice_in_dim(all_keys, block_id * rows_dev, rows_dev, 1)
        raw_scores = (
            jnp.einsum("bqhmd,bkhmd->bhmqk", queries, key_blk, preferred_element_type=jnp.float32)
            * scale
        )
        key_pos = block_id * rows_dev + jnp.arange(rows_dev, dtype=jnp.int32)
        scores = jnp.where(key_pos[None, :] <= query_pos[:, None], raw_scores, -jnp.inf)
        top_next = jnp.maximum(top_now, jnp.max(scores, axis=-1))
        total_next = total_now * jnp.exp(top_now - top_next) + jnp.sum(
            jnp.exp(scores - top_next[..., None]), axis=-1
        )
        score_store = lax.dynamic_update_index_in_dim(score_store, scores, block_id, 0)
        return (top_next, total_next, score_store)

    stat_shape = (groups, soft_heads, 2, query_rows)
    store_init = jnp.full((block_total,) + stat_shape + (rows_dev,), -jnp.inf, jnp.float32)
    top_all, total_all, score_store = lax.fori_loop(
        0,
        reach,
        first_pass,
        (
            jnp.full(stat_shape, -jnp.inf, jnp.float32),
            jnp.zeros(stat_shape, jnp.float32),
            store_init,
        ),
    )
    mass = top_all + jnp.log(total_all)

    def second_pass(block_id, accum):
        scores = lax.dynamic_index_in_dim(score_store, block_id, 0, keepdims=False)
        probs = jnp.exp(scores - top_all[..., None]) / total_all[..., None]
        weights = (probs[:, :, 0] - soft_lambda[None, :, None, None] * probs[:, :, 1]).astype(
            jnp.bfloat16
        )
        value_blk = lax.dynamic_slice_in_dim(all_values, block_id * rows_dev, rows_dev, 1)
        return accum + jnp.einsum(
            "bhqk,bkhv->bhqv", weights, value_blk, preferred_element_type=jnp.float32
        )

    accum = lax.fori_loop(
        0, reach, second_pass, jnp.zeros((groups, soft_heads, query_rows, DIFF_VALUE), jnp.float32)
    )
    soft_mix = scaled_rms(accum, soft_gain).astype(jnp.bfloat16).transpose(0, 2, 1, 3)
    soft_mix = soft_mix.reshape(groups, query_rows, soft_heads * DIFF_VALUE)
    return (soft_mix, mass)


def mixers(
    normed,
    shift_rows,
    lin_query,
    lin_key,
    lin_value,
    lin_decay,
    decay_bias,
    soft_query,
    soft_key,
    soft_value,
    soft_lambda,
    lin_gain,
    soft_gain,
):
    groups, rows_dev, model_width = normed.shape
    lin_heads = lin_query.shape[1] // GLA_KEY
    soft_heads = soft_value.shape[1] // DIFF_VALUE
    place = lax.axis_index(SP)
    shift_wide = shift_rows.astype(jnp.float32)
    lin_q = (
        project(normed, lin_query)
        .astype(jnp.bfloat16)
        .reshape(groups, rows_dev, lin_heads, GLA_KEY)
    )
    lin_k = (
        project(normed, lin_key).astype(jnp.bfloat16).reshape(groups, rows_dev, lin_heads, GLA_KEY)
    )
    lin_v = (
        project(normed, lin_value)
        .astype(jnp.bfloat16)
        .reshape(groups, rows_dev, lin_heads, GLA_VALUE)
    )
    gate_input = project(normed, lin_decay) + decay_bias + shift_wide[0][:, :, None]
    log_decay = jax.nn.log_sigmoid(gate_input) / decay_tau + shift_wide[1][:, :, None]
    log_decay = log_decay.reshape(groups, rows_dev, lin_heads, GLA_KEY)
    outs, carried, state_end, offset_end = block_pass(
        lin_q.astype(jnp.float32),
        lin_k.astype(jnp.float32),
        lin_v.astype(jnp.float32),
        log_decay,
        BLOCK,
    )
    keep_in, state_in = carried_in(
        (jnp.exp(offset_end), state_end),
        SP,
        chain_join,
        (jnp.ones_like(offset_end), jnp.zeros_like(state_end)),
    )
    outs = outs + jnp.einsum("nbhcd,bhdv->nbhcv", carried, state_in)
    lin_raw = outs.transpose(1, 0, 3, 2, 4).reshape(groups, rows_dev, lin_heads, GLA_VALUE)
    lin_mix = (
        scaled_rms(lin_raw, lin_gain)
        .astype(jnp.bfloat16)
        .reshape(groups, rows_dev, lin_heads * GLA_VALUE)
    )
    positions = place * rows_dev + jnp.arange(rows_dev, dtype=jnp.int32)
    soft_q = rotate(
        project(normed, soft_query)
        .astype(jnp.bfloat16)
        .reshape(groups, rows_dev, soft_heads, 2, DIFF_HEAD),
        positions,
    )
    soft_k = rotate(
        project(normed, soft_key)
        .astype(jnp.bfloat16)
        .reshape(groups, rows_dev, soft_heads, 2, DIFF_HEAD),
        positions,
    )
    soft_v = (
        project(normed, soft_value)
        .astype(jnp.bfloat16)
        .reshape(groups, rows_dev, soft_heads, DIFF_VALUE)
    )
    all_keys, all_values = (
        lax.all_gather(soft_k, SP, axis=1, tiled=True),
        lax.all_gather(soft_v, SP, axis=1, tiled=True),
    )
    soft_mix, mass = attend(
        soft_q, positions, place + 1, all_keys, all_values, soft_lambda, soft_gain, rows_dev
    )
    return (lin_mix, soft_mix, mass)


def output_term(lin_mix, soft_mix, lin_out, soft_out, rows_dev, parts):
    col_width = lin_out.shape[1] // parts

    def term(start, row_count):
        pieces = []
        for turn_index in range(row_count // rows_dev):
            piece_id = (start + turn_index * rows_dev) // rows_dev
            seq_id = piece_id // parts
            part_id = piece_id % parts
            lin_rows = lax.dynamic_index_in_dim(lin_mix, seq_id, 0, keepdims=False)
            soft_rows = lax.dynamic_index_in_dim(soft_mix, seq_id, 0, keepdims=False)
            lin_cols = lax.dynamic_slice_in_dim(lin_out, part_id * col_width, col_width, 1)
            soft_cols = lax.dynamic_slice_in_dim(soft_out, part_id * col_width, col_width, 1)
            pieces.append(
                jnp.dot(lin_rows, lin_cols, preferred_element_type=jnp.float32)
                + jnp.dot(soft_rows, soft_cols, preferred_element_type=jnp.float32)
            )
        return jnp.concatenate(pieces, axis=0)

    return term


def shards(
    tokens,
    norm_gain,
    lin_query,
    lin_key,
    lin_value,
    lin_decay,
    decay_bias,
    decay_shift,
    soft_query,
    soft_key,
    soft_value,
    soft_lambda,
    lin_gain,
    soft_gain,
    lin_out,
    soft_out,
):
    rows_dev = tokens.shape[1]
    parts = lax.axis_size("tp")
    fs_size = lax.axis_size("fs")
    fs_index = lax.axis_index("fs")
    tp_index = lax.axis_index("tp")
    whole = lax.all_gather(tokens, "tp", axis=2, tiled=True).astype(jnp.float32)
    normed = scaled_rms(whole, norm_gain).astype(jnp.bfloat16)
    lambda_grid = soft_lambda.reshape(fs_size, parts, -1)
    bias_grid = decay_bias.reshape(fs_size, parts, -1)
    all_rows, all_shift = (
        lax.all_gather(normed, "fs", axis=0, tiled=True),
        lax.all_gather(decay_shift, "fs", axis=1, tiled=True),
    )
    head_lambda = lax.dynamic_index_in_dim(
        lax.dynamic_index_in_dim(lambda_grid, fs_index, 0, keepdims=False),
        tp_index,
        0,
        keepdims=False,
    )
    head_bias = lax.dynamic_index_in_dim(
        lax.dynamic_index_in_dim(bias_grid, fs_index, 0, keepdims=False),
        tp_index,
        0,
        keepdims=False,
    )
    lin_mix, soft_mix, mass = mixers(
        all_rows,
        all_shift,
        lin_query,
        lin_key,
        lin_value,
        lin_decay,
        head_bias,
        soft_query,
        soft_key,
        soft_value,
        head_lambda,
        lin_gain,
        soft_gain,
    )
    term = output_term(lin_mix, soft_mix, lin_out, soft_out, rows_dev, parts)
    summed = lax.psum_scatter(
        term(jnp.int32(0), rows_dev * lax.axis_size(("fs", "tp"))).astype(jnp.bfloat16),
        ("fs", "tp"),
        scatter_dimension=0,
        tiled=True,
    ).astype(jnp.float32)
    log_mass = mass.transpose(1, 2, 0, 3)
    mixed = summed.astype(jnp.bfloat16).reshape(1, rows_dev, summed.shape[1])
    return (mixed, log_mass)


def solution(mesh):
    split = Mesh(
        mesh.devices.reshape(4, 4, mesh.shape["fs"], mesh.shape["tp"]), ("sp_0", "sp_1", "fs", "tp")
    )
    placed = (
        P("fs", SP, "tp"),
        P(),
        P(None, ("fs", "tp")),
        P(None, ("fs", "tp")),
        P(None, ("fs", "tp")),
        P(None, ("fs", "tp")),
        P(),
        P(None, "fs", SP),
        P(None, ("fs", "tp")),
        P(None, ("fs", "tp")),
        P(None, ("fs", "tp")),
        P(),
        P(),
        P(),
        P(("fs", "tp"), None),
        P(("fs", "tp"), None),
    )
    return jax.shard_map(
        shards,
        mesh=split,
        in_specs=placed,
        out_specs=(P("fs", SP, "tp"), P(("fs", "tp"), None, None, SP)),
        check_vma=False,
    )
```

profile of v0, /device:TPU:0, one launch (start us, length us, event | category | flops | bytes accessed | tf_op | source)
XLA Modules:
  0.0 483.6 jit_solution(4084504965831790650)
XLA Ops:
  8.0 15.9 %all-gather.10.cloned.1.call-done = bf16[1,256,2048]{2,1,0:T(8,128)(2,1)} async-done(((bf16[1,256,1024]{2,1,0:T(8,128)(2,1)}), bf16[1,256,2048]{2,1,0:T(8,128)(2,1)}) %all-gather.10.cloned.1.call-update) | async-done | bytes 1048592 | tf_op jit(solution)/shard_map/all_gather | solution.py:307
  25.4 2.6 fusion.48
  28.1 9.8 %all_gather.37 = bf16[2,4,256]{2,0,1:T(2,128)(2,1)S(1)} all-gather(bf16[2,1,256]{2,0,1:T(2,128)(2,1)S(1)} %copy-done.14), channel_id=1, replica_groups=mesh['sp_0'=4,'sp_1'=4,'fs'=4,'tp'=2] {'fs'}, dimensions={1}, use_global_device_ids=true | all-gather | bytes 5120 | tf_op jit(solution)/shard_map/all_gather | solution.py:313
  38.6 39.1 %all-gather.12.cloned.1.call-done = bf16[4,256,2048]{2,1,0:T(8,128)(2,1)} async-done(((bf16[1,256,2048]{2,1,0:T(8,128)(2,1)}), bf16[4,256,2048]{2,1,0:T(8,128)(2,1)}) %all-gather.12.cloned.1.call-update) | async-done | bytes 4194320 | tf_op jit(solution)/shard_map/all_gather | solution.py:312
  77.7 3.8 fusion.100
  85.5 21.9 %while.44 = (s32[]{:T(128)}, f32[4,1,128,256]{3,2,0,1:T(8,128)S(1)}, f32[4,1,128]{2,0,1:T(4,128)S(1)}, f32[4,4,1,64,256]{4,3,0,1,2:T(8,128)}, bf16[4,4,1,64,128]...) while((s32[]{:T(128)}, ...), condition=%wide.region_4.5_spmd.clone, body=%wide.region_1.4_spmd.clone.sunk | while | flops 55235584 | bytes 4980881 | solution.py:107
  85.8 3.7 multiply_reduce_fusion.3
  91.3 3.7 multiply_reduce_fusion.3
  96.7 3.7 multiply_reduce_fusion.3
  102.2 3.7 multiply_reduce_fusion.3
  108.8 11.1 %all-gather = bf16[16,1,128]{2,1,0:T(2,128)(2,1)S(1)} all-gather(bf16[4,1,128]{2,1,0:T(2,128)(2,1)S(1)} %copy.118), channel_id=2, replica_groups=mesh['sp_0'=4,'sp_1'=4,'fs'=4,'tp'=2] {'sp_1'}, dimensions={0}, use_global_device_ids=true | all-gather | bytes 5120 | tf_op jit(solution)/shard_map/all_gather | solution.py:30
  120.0 12.8 %all-gather.18.cloned.1.call-done = bf16[16,1,128,256]{3,2,1,0:T(8,128)(2,1)} async-done(((bf16[4,1,128,256]{3,2,1,0:T(8,128)(2,1)}), bf16[16,1,128,256]{3,2,1,0:T(8,128)(2,1)}) %all-gather.18.cloned.1.call-update) | async-done | bytes 1048592 | tf_op jit(solution)/shard_map/all_gather | solution.py:30
  132.8 2.2 fusion.153
  135.3 3.8 convolution_convert_fusion.2
  139.9 3.8 convolution_convert_fusion.1
  146.2 2.5 copy.161
  148.6 2.8 subtract_convert_fusion
  152.6 4.7 convolution_convert_fusion
  158.2 10.1 %all_gather.40 = bf16[4,4,1,128]{3,1,2,0:T(4,128)(2,1)S(1)} all-gather(bf16[1,4,1,128]{3,1,2,0:T(4,128)(2,1)S(1)} %fusion.174), channel_id=1, replica_groups=mesh['sp_0'=4,'sp_1'=4,'fs'=4,'tp'=2] {'sp_0'}, dimensions={0}, use_global_device_ids=true | all-gather | bytes 5120 | tf_op jit(solution)/shard_map/all_gather | solution.py:30
  168.7 3.6 fusion.73
  184.2 48.9 %all-gather.16.cloned.1.call-done = bf16[4,4096,1,2,128]{4,1,3,0,2:T(8,128)(2,1)} async-done(((bf16[4,256,1,2,128]{4,1,3,0,2:T(8,128)(2,1)}), bf16[4,4096,1,2,128]{4,1,3,0,2:T(8,128)(2,1)}) %all-gather.16.cloned.1.call-update) | async-done | bytes 8388624 | tf_op jit(solution)/shard_map/all_gather | solution.py:253
  233.1 11.3 %broadcast_in_dim.60 = f32[16,4,1,2,256,256]{4,5,3,1,2,0:T(8,128)} broadcast(f32[]{:T(128)} %constant.670.clone.1), dimensions={} | broadcast | bytes 33554436 | tf_op jit(solution)/shard_map/broadcast_in_dim | solution.py:146
  244.4 3.6 while.43
  246.1 1.6 bitcast_dynamic-update-slice_fusion.2
  248.7 57.0 %all-gather.20.cloned.1.call-done = bf16[4,4096,256]{2,1,0:T(8,128)(2,1)} async-done(((bf16[4,256,256]{2,1,0:T(8,128)(2,1)}), bf16[4,4096,256]{2,1,0:T(8,128)(2,1)}) %all-gather.20.cloned.1.call-update) | async-done | bytes 8388624 | tf_op jit(solution)/shard_map/all_gather | solution.py:254
  305.8 7.7 %while.42 = (s32[]{:T(128)}, f32[4,1,256,256]{3,2,0,1:T(8,128)S(1)}, s32[]{:T(128)}, f32[16,4,1,2,256,256]{4,5,3,1,2,0:T(8,128)}, f32[4,1,2,256]{3,0,2,1:T(4,128...) while((s32[]{:T(128)}, ...), condition=%wide.region_11.12_spmd, body=%wide.region_10.11_spmd.sunk | while | flops 136314880 | bytes 17318612 | solution.py:170
  305.8 1.8 constant_dynamic-slice_fusion.3
  307.6 1.9 copy.191
  309.5 1.9 fusion.213
  311.4 2.0 fusion.214
  314.0 2.7 fusion.51
  324.5 152.2 %reduce-scatter.2.cloned.1.call-done = bf16[256,1024]{1,0:T(8,128)(2,1)} async-done(((bf16[2048,1024]{1,0:T(8,128)(2,1)}), bf16[256,1024]{1,0:T(8,128)(2,1)}) %reduce-scatter.2.cloned.1.call-update) | async-done | bytes 524304 | tf_op jit(solution)/shard_map/reduce_scatter | solution.py:343
  (174 shorter events, 43.7 us)
Async XLA Ops:
  7.2 74.3 %copy-start = (bf16[2048,256]{1,0:T(8,128)(2,1)S(1)}, bf16[2048,256]{1,0:T(8,128)(2,1)}, u32[]{:S(2)}) copy-start(bf16[2048,256]{1,0:T(8,128)(2,1)} %param.26) | copy-start | bytes 3145732
  7.2 20.9 %copy-start.14 = (bf16[2,1,256]{2,0,1:T(2,128)(2,1)S(1)}, bf16[2,1,256]{2,0,1:T(2,128)(2,1)}, u32[]{:S(2)}) copy-start(bf16[2,1,256]{2,0,1:T(2,128)(2,1)} %param.29) | copy-start | bytes 3076
  7.2 70.5 %copy-start.19 = (bf16[2048,128]{1,0:T(8,128)(2,1)S(1)}, bf16[2048,128]{1,0:T(8,128)(2,1)}, u32[]{:S(2)}) copy-start(bf16[2048,128]{1,0:T(8,128)(2,1)} %param.27) | copy-start | bytes 1572868
  7.2 16.7 %all-gather.10.cloned.1.call-start = ((), (), s32[]{:S(2)}) async-start(), calls=%async_computation.1 | async-start | bytes 1572864 | tf_op jit(solution)/shard_map/all_gather | solution.py:307
  7.9 69.7 %all-gather.12.cloned.1.call-start = ((), (), s32[]{:S(2)}) async-start(), calls=%async_computation.2 | async-start | bytes 5242880 | tf_op jit(solution)/shard_map/all_gather | solution.py:312
  28.0 104.8 %all-gather.18.cloned.1.call-start = ((), (), s32[]{:S(2)}) async-start(), calls=%async_computation.6 | async-start | bytes 1310720 | tf_op jit(solution)/shard_map/all_gather | solution.py:30
  77.7 3.8 copy-start.18
  81.5 1.3 copy-start.20
  82.8 1.3 copy-start.21
  107.4 0.8 copy-start.22
  108.2 60.5 %all-gather.14.cloned.1.call-start = ((), (), s32[]{:S(2)}) async-start(), calls=%async_computation.3 | async-start | bytes 1310720 | tf_op jit(solution)/shard_map/all_gather | solution.py:30
  135.1 98.0 %all-gather.16.cloned.1.call-start = ((), (), s32[]{:S(2)}) async-start(), calls=%async_computation.4 | async-start | bytes 8912896 | tf_op jit(solution)/shard_map/all_gather | solution.py:253
  152.5 4.9 %copy-start.17 = (f32[8]{0:T(128)S(1)}, f32[8]{0:T(128)}, u32[]{:S(2)}) copy-start(f32[8]{0:T(128)} %param.33) | copy-start | bytes 100
  152.5 15.8 %copy-start.11 = (bf16[4,256,1,2,64]{4,1,3,0,2:T(8,128)(2,1)S(1)}, bf16[4,256,1,2,64]{4,1,3,0,2:T(8,128)(2,1)}, u32[]{:S(2)}) copy-start(bf16[4,256,1,2,64]{4,1,3,0,2:T(8,128)(2,1)} %get-tuple-element.303) | copy-start | bytes 786436
  152.5 15.8 %copy-start.12 = (bf16[4,256,1,2,64]{4,1,3,0,2:T(8,128)(2,1)S(1)}, bf16[4,256,1,2,64]{4,1,3,0,2:T(8,128)(2,1)}, u32[]{:S(2)}) copy-start(bf16[4,256,1,2,64]{4,1,3,0,2:T(8,128)(2,1)} %get-tuple-element.304) | copy-start | bytes 786436
  152.6 16.1 %copy-start.13 = (bf16[16,1,128,256]{3,2,1,0:T(8,128)(2,1)S(1)}, bf16[16,1,128,256]{3,2,1,0:T(8,128)(2,1)}, u32[]{:S(2)}) copy-start(bf16[16,1,128,256]{3,2,1,0:T(8,128)(2,1)} %all-gather.18.cloned.1.call-done) | copy-start | bytes 3145732
  152.6 153.1 %all-gather.20.cloned.1.call-start = ((), (), s32[]{:S(2)}) async-start(), calls=%async_computation.7 | async-start | bytes 8912896 | tf_op jit(solution)/shard_map/all_gather | solution.py:254
  157.4 15.1 %copy-start.15 = (f32[256]{0:T(256)S(1)}, f32[256]{0:T(256)}, u32[]{:S(2)}) copy-start(f32[256]{0:T(256)} %param.34) | copy-start | bytes 3076
  157.4 319.3 %reduce-scatter.2.cloned.1.call-start = ((), (), s32[]{:S(2)}) async-start(), calls=%async_computation.5 | async-start | bytes 4718592 | tf_op jit(solution)/shard_map/reduce_scatter | solution.py:343
  168.6 5.3 %copy-start.3 = (bf16[256,2048]{1,0:T(8,128)(2,1)S(1)}, bf16[256,2048]{1,0:T(8,128)(2,1)}, u32[]{:S(2)}) copy-start(bf16[256,2048]{1,0:T(8,128)(2,1)} %param.36) | copy-start | bytes 3145732
  305.7 8.0 %copy-start.16 = (f32[256]{0:T(256)S(1)}, f32[256]{0:T(256)}, u32[]{:S(2)}) copy-start(f32[256]{0:T(256)} %param.35) | copy-start | bytes 3076
  313.5 3.2 copy-start.2
  313.5 3.2 copy-start.10
  313.5 4.3 copy-start.9
  313.7 5.2 %copy-start.8 = (f32[256,1024]{1,0:T(8,128)S(1)}, f32[256,1024]{1,0:T(8,128)}, u32[]{:S(2)}) copy-start(f32[256,1024]{1,0:T(8,128)} %fusion.127) | copy-start | bytes 3145732
  314.0 6.1 %copy-start.7 = (f32[256,1024]{1,0:T(8,128)S(1)}, f32[256,1024]{1,0:T(8,128)}, u32[]{:S(2)}) copy-start(f32[256,1024]{1,0:T(8,128)} %fusion.137) | copy-start | bytes 3145732
  316.7 4.5 copy-start.6
  317.8 4.4 copy-start.5
  318.9 4.4 copy-start.4
  321.2 155.6 %copy-start.1 = (bf16[2048,256]{1,0:T(8,128)(2,1)S(1)}, bf16[2048,256]{1,0:T(8,128)(2,1)}, u32[]{:S(2)}) copy-start(bf16[2048,256]{1,0:T(8,128)(2,1)} %param.26) | copy-start | bytes 3145732
Sparse Core Ops, SparseCore 0:
  9.7 14.1 all-gather.9
  28.1 49.5 all-gather.11
  108.3 24.4 all-gather.17
  135.2 24.6 all-gather.13
  161.9 71.1 all-gather.15
  235.1 70.5 all-gather.19
  324.6 152.0 reduce-scatter.1
where the time goes:
time: 487 us; the launch traced here: 484 us
  waiting for transfers between devices  327 us (67%)
  matrix products  53.4 us (11%)
  other arithmetic  32.7 us (7%)
  blocking collectives  31.1 us (6%)
  local copies, waits for them, and re-layouts  24.3 us (5%)
  between operations  14.7 us (3%)
    reduce_scatter x1, waiting for transfers between devices, shards(): lax.psum_scatter(term(jnp.int32(0), rows_dev * lax.axis_size(('fs', 'tp')...  152 us
    all_gather x1, waiting for transfers between devices, mixers(): lax.all_gather(soft_v, SP, axis=1, tiled=True)  57 us
    all_gather x1, waiting for transfers between devices, mixers(): lax.all_gather(soft_k, SP, axis=1, tiled=True)  48.9 us
    all_gather x1, waiting for transfers between devices, shards(): lax.all_gather(normed, 'fs', axis=0, tiled=True)  39.1 us
    all_gather x2, blocking collectives, carried_in(): lax.all_gather(part.astype(kind), axis)  21.3 us
    dot_general x7, matrix products, project(): product = jnp.dot(flat_rows, weight, preferred_element_type=jnp.float32)  19.8 us
    all_gather x1, waiting for transfers between devices, shards(): whole = lax.all_gather(tokens, 'tp', axis=2, tiled=True).astype(jnp.float32)  15.9 us
    reduce_sum x4, other arithmetic, advance(): jnp.sum(query_blk[:, :, :, None, :] * key_blk[:, :, None, :, :] * decay_p...  14.9 us
  transfers between devices with their start and end apart: 7, of which 6 were waited for; matrix products, arithmetic and copies ran while one was open for 11% of the time, Pallas kernels for 0%

commit v1 on v0

--- a/solution.py
+++ b/solution.py
@@ -13,6 +13,13 @@
 norm_eps = 1e-06
 decay_tau = 16.0
 rope_base = 500000.0
+
+
+def gather_over(block, name, dim):
+    devices = lax.axis_size(name)
+    blocks = jnp.stack([block for _ in range(devices)])
+    blocks = lax.all_to_all(blocks, name, split_axis=0, concat_axis=0)
+    return jnp.concatenate(blocks, axis=dim)
 
 
 def neutral_like(array, identity):
@@ -250,7 +257,7 @@
         .reshape(groups, rows_dev, soft_heads, DIFF_VALUE)
     )
     all_keys, all_values = (
-        lax.all_gather(soft_k, SP, axis=1, tiled=True),
+        gather_over(soft_k, SP, 1),
         lax.all_gather(soft_v, SP, axis=1, tiled=True),
     )
     soft_mix, mass = attend(

time: 487 us -> 565 us (1.16)
  blocking collectives: 31.1 us -> 113 us
  waiting for transfers between devices: 327 us -> 306 us
  local copies, waits for them, and re-layouts: 24.3 us -> 37.1 us
  starting transfers between devices: 0.47 us -> 6.74 us
    all_gather x2, blocking collectives: 21.3 us -> 103 us  [carried_in(): lax.all_gather(part.astype(kind), axis)]
    all_gather x1, waiting for transfers between devices: 57 us -> 0.01 us  [mixers(): lax.all_gather(soft_v, SP, axis=1, tiled=True)]
    all_gather x1 -> x0, waiting for transfers between devices: 48.9 us -> none  [mixers(): lax.all_gather(soft_k, SP, axis=1, tiled=True)]
    reduce_scatter x1, waiting for transfers between devices: 152 us -> 198 us  [shards(): lax.psum_scatter(term(jnp.int32(0), rows_dev * lax.axis_size(('fs', 'tp')...]
    all_to_all x0 -> x1, waiting for transfers between devices: none -> 39.2 us  [gather_over(): blocks = lax.all_to_all(blocks, name, split_axis=0, concat_axis=0)]
    all_to_all x0 -> x1, local copies, waits for them, and re-layouts: none -> 7.72 us  [gather_over(): blocks = lax.all_to_all(blocks, name, split_axis=0, concat_axis=0)]
    all_to_all x0 -> x1, starting transfers between devices: none -> 6.32 us  [gather_over(): blocks = lax.all_to_all(blocks, name, split_axis=0, concat_axis=0)]
  transfers between devices with their start and end apart: 7 -> 7, of which waited for: 6 -> 5; matrix products, arithmetic and copies ran while one was open for 11% -> 12% of each run, Pallas kernels for 0% -> 0%
where the time goes in v1:
time: 565 us; the launch traced here: 562 us
  waiting for transfers between devices  306 us (54%)
  blocking collectives  113 us (20%)
  matrix products  53 us (9%)
  local copies, waits for them, and re-layouts  37.1 us (7%)
  other arithmetic  31.8 us (6%)
  between operations  14.7 us (3%)
  starting transfers between devices  6.74 us (1%)
    reduce_scatter x1, waiting for transfers between devices, shards(): lax.psum_scatter(term(jnp.int32(0), rows_dev * lax.axis_size(('fs', 'tp')...  198 us
    all_gather x2, blocking collectives, carried_in(): lax.all_gather(part.astype(kind), axis)  103 us
    all_to_all x1, waiting for transfers between devices, gather_over(): blocks = lax.all_to_all(blocks, name, split_axis=0, concat_axis=0)  39.2 us
    all_gather x1, waiting for transfers between devices, shards(): lax.all_gather(normed, 'fs', axis=0, tiled=True)  39.1 us
    dot_general x7, matrix products, project(): product = jnp.dot(flat_rows, weight, preferred_element_type=jnp.float32)  19.5 us
    all_gather x1, waiting for transfers between devices, shards(): whole = lax.all_gather(tokens, 'tp', axis=2, tiled=True).astype(jnp.float32)  15.9 us
    reduce_sum x4, other arithmetic, advance(): jnp.sum(query_blk[:, :, :, None, :] * key_blk[:, :, None, :, :] * decay_p...  14.9 us
    all_gather x2, waiting for transfers between devices, carried_in(): lax.all_gather(part.astype(kind), axis)  13.3 us
  transfers between devices with their start and end apart: 7, of which 5 were waited for; matrix products, arithmetic and copies ran while one was open for 12% of the time, Pallas kernels for 0%

profile of v1, /device:TPU:0, one launch (start us, length us, event | category | flops | bytes accessed | tf_op | source)
XLA Modules:
  0.0 562.1 jit_solution(13624261122700873347)
XLA Ops:
  8.0 15.9 %all-gather.9.cloned.1.call-done = bf16[1,256,2048]{2,1,0:T(8,128)(2,1)} async-done(((bf16[1,256,1024]{2,1,0:T(8,128)(2,1)}), bf16[1,256,2048]{2,1,0:T(8,128)(2,1)}) %all-gather.9.cloned.1.call-update) | async-done | bytes 1048592 | tf_op jit(solution)/shard_map/all_gather | solution.py:314
  25.4 2.6 fusion.48
  28.1 9.8 %all_gather.34 = bf16[2,4,256]{2,0,1:T(2,128)(2,1)S(1)} all-gather(bf16[2,1,256]{2,0,1:T(2,128)(2,1)S(1)} %copy-done.14), channel_id=1, replica_groups=mesh['sp_0'=4,'sp_1'=4,'fs'=4,'tp'=2] {'fs'}, dimensions={1}, use_global_device_ids=true | all-gather | bytes 5120 | tf_op jit(solution)/shard_map/all_gather | solution.py:320
  38.6 39.1 %all-gather.11.cloned.1.call-done = bf16[4,256,2048]{2,1,0:T(8,128)(2,1)} async-done(((bf16[1,256,2048]{2,1,0:T(8,128)(2,1)}), bf16[4,256,2048]{2,1,0:T(8,128)(2,1)}) %all-gather.11.cloned.1.call-update) | async-done | bytes 4194320 | tf_op jit(solution)/shard_map/all_gather | solution.py:319
  77.7 3.8 fusion.102
  85.5 21.9 %while.44 = (s32[]{:T(128)}, f32[4,1,128,256]{3,2,0,1:T(8,128)S(1)}, f32[4,1,128]{2,0,1:T(4,128)S(1)}, f32[4,4,1,64,256]{4,3,0,1,2:T(8,128)}, bf16[4,4,1,64,128]...) while((s32[]{:T(128)}, ...), condition=%wide.region_4.5_spmd.clone, body=%wide.region_1.4_spmd.clone.sunk | while | flops 55235584 | bytes 4980881 | solution.py:114
  85.8 3.7 multiply_reduce_fusion.3
  91.3 3.7 multiply_reduce_fusion.3
  96.7 3.7 multiply_reduce_fusion.3
  102.2 3.7 multiply_reduce_fusion.3
  108.3 11.1 %all-gather = bf16[16,1,128]{2,1,0:T(2,128)(2,1)S(1)} all-gather(bf16[4,1,128]{2,1,0:T(2,128)(2,1)S(1)} %copy.151), channel_id=2, replica_groups=mesh['sp_0'=4,'sp_1'=4,'fs'=4,'tp'=2] {'sp_1'}, dimensions={0}, use_global_device_ids=true | all-gather | bytes 5120 | tf_op jit(solution)/shard_map/all_gather | solution.py:37
  119.5 13.3 %all-gather.15.cloned.1.call-done = bf16[16,1,128,256]{3,2,1,0:T(8,128)(2,1)} async-done(((bf16[4,1,128,256]{3,2,1,0:T(8,128)(2,1)}), bf16[16,1,128,256]{3,2,1,0:T(8,128)(2,1)}) %all-gather.15.cloned.1.call-update) | async-done | bytes 1048592 | tf_op jit(solution)/shard_map/all_gather | solution.py:37
  132.8 2.2 fusion.155
  135.9 3.8 convolution_convert_fusion.2
  140.4 4.6 convolution_convert_fusion
  145.1 3.6 convolution_convert_fusion.1
  151.1 2.4 copy.195
  153.5 2.7 subtract_convert_fusion
  156.5 5.3 stack.2
  161.9 6.3 %all-to-all-start = ((bf16[16,4,256,1,2,128]{5,2,4,1,3,0:T(8,128)(2,1)}), bf16[16,4,256,1,2,128]{5,2,4,1,3,0:T(8,128)(2,1)}, u32[]{:S(2)}, u32[]{:S(2)}) async-start(bf16[16,4,256,1,2,128]{5,2,4,1,3,0:T(8,128)(2,1)} %stack.2), calls=%async_computation | async-start | bytes 16777216 | tf_op jit(solution)/shard_map/all_to_all | solution.py:21
  169.0 91.7 %all_gather.37 = bf16[4,4,1,128]{3,1,2,0:T(4,128)(2,1)S(1)} all-gather(bf16[1,4,1,128]{3,1,2,0:T(4,128)(2,1)S(1)} %fusion.176), channel_id=1, replica_groups=mesh['sp_0'=4,'sp_1'=4,'fs'=4,'tp'=2] {'sp_0'}, dimensions={0}, use_global_device_ids=true | all-gather | bytes 5120 | tf_op jit(solution)/shard_map/all_gather | solution.py:37
  261.1 3.6 fusion.73
  276.5 39.2 %all-to-all-done = bf16[16,4,256,1,2,128]{5,2,4,1,3,0:T(8,128)(2,1)} async-done(((bf16[16,4,256,1,2,128]{5,2,4,1,3,0:T(8,128)(2,1)}), bf16[16,4,256,1,2,128]{5,2,4,1,3,0:T(8,128)(2,1)}, u32[]{:S(2)}, u32[]{:S(2)}) %all-to-all-start) | async-done | bytes 8388640 | tf_op jit(solution)/shard_map/all_to_all | solution.py:21
  315.8 7.7 %copy.170 = bf16[16,4,256,1,2,128]{5,2,0,4,1,3:T(8,128)(2,1)} copy(bf16[16,4,256,1,2,128]{5,2,4,1,3,0:T(8,128)(2,1)} %all-to-all-done) | data formatting | bytes 16777216 | tf_op jit(solution)/shard_map/all_to_all | solution.py:21
  323.5 11.1 %broadcast_in_dim.60 = f32[16,4,1,2,256,256]{4,5,3,1,2,0:T(8,128)} broadcast(f32[]{:T(128)} %constant.670.clone.1), dimensions={} | broadcast | bytes 33554436 | tf_op jit(solution)/shard_map/broadcast_in_dim | solution.py:153
  334.6 3.6 while.43
  339.0 7.7 %while.42 = (s32[]{:T(128)}, f32[4,1,256,256]{3,2,0,1:T(8,128)S(1)}, s32[]{:T(128)}, f32[16,4,1,2,256,256]{4,5,3,1,2,0:T(8,128)}, f32[4,1,2,256]{3,0,2,1:T(4,128...) while((s32[]{:T(128)}, ...), condition=%wide.region_11.12_spmd, body=%wide.region_10.11_spmd.sunk | while | flops 136314880 | bytes 17318612 | solution.py:177
  340.8 1.9 copy.225
  342.7 1.9 fusion.215
  344.6 2.0 fusion.216
  347.2 2.7 fusion.51
  357.7 197.6 %reduce-scatter.2.cloned.1.call-done = bf16[256,1024]{1,0:T(8,128)(2,1)} async-done(((bf16[2048,1024]{1,0:T(8,128)(2,1)}), bf16[256,1024]{1,0:T(8,128)(2,1)}) %reduce-scatter.2.cloned.1.call-update) | async-done | bytes 524304 | tf_op jit(solution)/shard_map/reduce_scatter | solution.py:350
  (177 shorter events, 46.1 us)
Async XLA Ops:
  7.2 74.3 %copy-start = (bf16[2048,256]{1,0:T(8,128)(2,1)S(1)}, bf16[2048,256]{1,0:T(8,128)(2,1)}, u32[]{:S(2)}) copy-start(bf16[2048,256]{1,0:T(8,128)(2,1)} %param.26) | copy-start | bytes 3145732
  7.2 20.9 %copy-start.14 = (bf16[2,1,256]{2,0,1:T(2,128)(2,1)S(1)}, bf16[2,1,256]{2,0,1:T(2,128)(2,1)}, u32[]{:S(2)}) copy-start(bf16[2,1,256]{2,0,1:T(2,128)(2,1)} %param.29) | copy-start | bytes 3076
  7.2 70.5 %copy-start.20 = (bf16[2048,128]{1,0:T(8,128)(2,1)S(1)}, bf16[2048,128]{1,0:T(8,128)(2,1)}, u32[]{:S(2)}) copy-start(bf16[2048,128]{1,0:T(8,128)(2,1)} %param.27) | copy-start | bytes 1572868
  7.2 16.7 %all-gather.9.cloned.1.call-start = ((), (), s32[]{:S(2)}) async-start(), calls=%async_computation.2 | async-start | bytes 1572864 | tf_op jit(solution)/shard_map/all_gather | solution.py:314
  7.9 69.7 %all-gather.11.cloned.1.call-start = ((), (), s32[]{:S(2)}) async-start(), calls=%async_computation.3 | async-start | bytes 5242880 | tf_op jit(solution)/shard_map/all_gather | solution.py:319
  28.0 104.8 %all-gather.15.cloned.1.call-start = ((), (), s32[]{:S(2)}) async-start(), calls=%async_computation.6 | async-start | bytes 1310720 | tf_op jit(solution)/shard_map/all_gather | solution.py:37
  77.7 3.8 copy-start.18
  81.5 1.3 copy-start.21
  82.8 1.3 copy-start.22
  107.4 0.9 copy-start.23
  108.2 152.9 %all-gather.13.cloned.1.call-start = ((), (), s32[]{:S(2)}) async-start(), calls=%async_computation.4 | async-start | bytes 1310720 | tf_op jit(solution)/shard_map/all_gather | solution.py:37
  135.1 203.8 %all-gather.17.cloned.1.call-start = ((), (), s32[]{:S(2)}) async-start(), calls=%async_computation.7 | async-start | bytes 8912896 | tf_op jit(solution)/shard_map/all_gather | solution.py:261
  140.4 4.7 copy-start.19
  161.9 6.4 %copy-start.17 = (f32[8]{0:T(128)S(1)}, f32[8]{0:T(128)}, u32[]{:S(2)}) copy-start(f32[8]{0:T(128)} %param.33) | copy-start | bytes 100
  161.9 98.9 %copy-start.11 = (bf16[4,256,1,2,64]{4,1,3,0,2:T(8,128)(2,1)S(1)}, bf16[4,256,1,2,64]{4,1,3,0,2:T(8,128)(2,1)}, u32[]{:S(2)}) copy-start(bf16[4,256,1,2,64]{4,1,3,0,2:T(8,128)(2,1)} %get-tuple-element.311) | copy-start | bytes 786436
  161.9 98.9 %copy-start.12 = (bf16[4,256,1,2,64]{4,1,3,0,2:T(8,128)(2,1)S(1)}, bf16[4,256,1,2,64]{4,1,3,0,2:T(8,128)(2,1)}, u32[]{:S(2)}) copy-start(bf16[4,256,1,2,64]{4,1,3,0,2:T(8,128)(2,1)} %get-tuple-element.312) | copy-start | bytes 786436
  161.9 99.2 %copy-start.13 = (bf16[16,1,128,256]{3,2,1,0:T(8,128)(2,1)S(1)}, bf16[16,1,128,256]{3,2,1,0:T(8,128)(2,1)}, u32[]{:S(2)}) copy-start(bf16[16,1,128,256]{3,2,1,0:T(8,128)(2,1)} %all-gather.15.cloned.1.call-done) | copy-start | bytes 3145732
  161.9 153.9 %all-to-all-start = ((bf16[16,4,256,1,2,128]{5,2,4,1,3,0:T(8,128)(2,1)}), bf16[16,4,256,1,2,128]{5,2,4,1,3,0:T(8,128)(2,1)}, u32[]{:S(2)}, u32[]{:S(2)}) async-start(bf16[16,4,256,1,2,128]{5,2,4,1,3,0:T(8,128)(2,1)} %stack.2), calls=%async_computation | async-start | bytes 16777216 | tf_op jit(solution)/shard_map/all_to_all | solution.py:21
  168.2 96.6 %copy-start.15 = (f32[256]{0:T(256)S(1)}, f32[256]{0:T(256)}, u32[]{:S(2)}) copy-start(f32[256]{0:T(256)} %param.34) | copy-start | bytes 3076
  168.2 387.1 %reduce-scatter.2.cloned.1.call-start = ((), (), s32[]{:S(2)}) async-start(), calls=%async_computation.5 | async-start | bytes 4718592 | tf_op jit(solution)/shard_map/reduce_scatter | solution.py:350
  261.0 5.2 copy-start.3
  338.9 8.0 %copy-start.16 = (f32[256]{0:T(256)S(1)}, f32[256]{0:T(256)}, u32[]{:S(2)}) copy-start(f32[256]{0:T(256)} %param.35) | copy-start | bytes 3076
  346.7 3.2 copy-start.2
  346.7 3.2 copy-start.10
  346.7 4.3 copy-start.9
  346.9 5.2 copy-start.8
  347.2 6.1 %copy-start.7 = (f32[256,1024]{1,0:T(8,128)S(1)}, f32[256,1024]{1,0:T(8,128)}, u32[]{:S(2)}) copy-start(f32[256,1024]{1,0:T(8,128)} %fusion.139) | copy-start | bytes 3145732
  349.9 4.5 copy-start.6
  351.0 4.4 copy-start.5
  352.1 4.4 copy-start.4
  354.4 200.9 %copy-start.1 = (bf16[2048,256]{1,0:T(8,128)(2,1)S(1)}, bf16[2048,256]{1,0:T(8,128)(2,1)}, u32[]{:S(2)}) copy-start(bf16[2048,256]{1,0:T(8,128)(2,1)} %param.26) | copy-start | bytes 3145732
Sparse Core Ops, SparseCore 0:
  9.7 14.1 all-gather.8
  28.1 49.5 all-gather.10
  108.3 24.4 all-gather.14
  135.2 24.6 all-gather.12
  161.9 163.6 all-gather.16
  357.8 197.4 reduce-scatter.1
